TPU v7x, 512 devices: a 4x2x32 block of a 4x8x32 slice. The times are simulated.
512 devices in a mesh: grp: 2 (over y), sp: 64 (over z, core), tp: 4 (over x).
Axes of the slice: x: 4, y: 2, z: 32, core: 2. Of those that a mesh axis runs over, the one named last changes fastest.
The devices are a block of a 4x8x32 slice.
Arguments:
- recurrent_query: bfloat16 [32768, 1024], P(('grp', 'sp'), 'tp'), parts along dimension 0, may hold values from -6 to 6
- recurrent_forget_gate: bfloat16 [32768, 1024], P(('grp', 'sp'), 'tp'), parts along dimension 0, may hold values from -4.5 to 4.5
- recurrent_value: bfloat16 [32768, 1024], P(('grp', 'sp'), 'tp'), parts along dimension 0, may hold values from -6 to 6
- recurrent_gate_lower_bound: float32 [1024], P('tp'), may hold values from 1.5 to 14
- recurrent_added_decay: float32 [32768, 8], P(('grp', 'sp'), 'tp'), parts along dimension 0, may hold values from -0.51 to 0
- recurrent_norm_gain: float32 [128], replicated, may hold values from 0.1 to 1.9
- attention_query_first: bfloat16 [32768, 512], P(('grp', 'sp'), 'tp'), parts along dimension 0, may hold values from -20 to 20
- attention_key_first: bfloat16 [32768, 256], P(('grp', 'sp'), 'tp'), parts along dimension 0, may hold values from -20 to 20
- attention_query_second: bfloat16 [32768, 512], P(('grp', 'sp'), 'tp'), parts along dimension 0, may hold values from -20 to 20
- attention_key_second: bfloat16 [32768, 256], P(('grp', 'sp'), 'tp'), parts along dimension 0, may hold values from -20 to 20
- attention_value: bfloat16 [32768, 512], P(('grp', 'sp'), 'tp'), parts along dimension 0, may hold values from -6 to 6
- second_map_weight: float32 [8], P('tp'), may hold values from 0.3 to 0.8
- attention_norm_gain: float32 [128], replicated, may hold values from 0.1 to 1.9
- output_weight: bfloat16 [2, 1024, 2048], P(None, 'tp', 'sp'), may hold values from -0.125 to 0.125
Outputs:
- mixed: bfloat16 [32768, 2048], P(('grp', 'sp', 'tp')), parts along dimension 0
There are 2 independent parts, one for each index of `grp`. A program takes and returns all parts, laid end to end along the dimension named above; an argument that names none is the same for every part. Nothing has to cross between parts.
All inputs are finite; a program needn't handle non-finite values.
Results may differ from a plain program's by a relative error of at most 0.02.
Values may be sent and summed in bfloat16 or wider, within the bound.
A program may use at most 64 MiB of HBM per device.

v0:
```python
import jax
import jax.numpy as jnp
from jax import lax
from jax.sharding import PartitionSpec as P

HG_DK = 128
HG_DV = 128
DA_HD = 64
BLK = 32


epsilon = 1e-06
key_span = 512


def carried_in(array, axis, combine, identity):
    size, place = (lax.axis_size(axis), lax.axis_index(axis))
    everything = jax.tree.map(
        lambda part, kind: lax.all_gather(part.astype(kind), axis),
        array,
        (jnp.bfloat16, jnp.bfloat16),
    )
    start = jax.tree.map(
        lambda part, zero: jnp.broadcast_to(jnp.asarray(zero, part.dtype), part.shape),
        array,
        identity,
    )

    def hop(k, before):
        reached = k < place
        new = combine(
            before, jax.tree.map(lambda part, own: part[k].astype(own.dtype), everything, array)
        )
        return jax.tree.map(lambda a, b: jnp.where(reached, a, b), new, before)

    return lax.fori_loop(0, size, hop, start)


def in_one_piece(arrays, axis, dim, along):
    ends, at = ([], 0)
    for a in arrays[:-1]:
        at += a.shape[along]
        ends.append(at)
    both = jnp.concatenate(arrays, axis=along)
    return tuple(jnp.split(lax.all_gather(both, axis, axis=dim, tiled=True), ends, axis=along))


def split_up(array, dim, size):
    before, after = (array.shape[:dim], array.shape[dim + 1 :])
    return jnp.moveaxis(array.reshape(*before, size, -1, *after), dim, 0)


def summed_on_arrival(array, axis, dim):
    size = lax.axis_size(axis)
    pieces = lax.all_to_all(split_up(array, dim, size), axis, 0, 0, tiled=True)
    return jnp.sum(pieces.astype(jnp.float32), axis=0)


def head_norm(head_values, gain_vec):
    mean_square = jnp.mean(head_values * head_values, axis=-1, keepdims=True)
    return head_values * lax.rsqrt(mean_square + epsilon) * gain_vec


def decay_factors(gate_preactivation, lower_bound_logit, added_log_decay, number_of_heads):
    token_count = gate_preactivation.shape[0]
    floor_rate = jax.nn.sigmoid(-lower_bound_logit).reshape(number_of_heads, -1)
    state_inflow = floor_rate[None] * jax.nn.sigmoid(
        -gate_preactivation.astype(jnp.float32)
    ).reshape(token_count, number_of_heads, -1)
    decay_logarithm = jnp.log1p(-state_inflow) + added_log_decay[:, :, None]
    return (state_inflow, decay_logarithm)


def recurrence_blocks(queries, decay_logarithm, state_inflow, value_rows, block_len):
    token_count, number_of_heads, key_width = queries.shape
    block_count = token_count // block_len

    def to_blocks(source):
        return source.reshape(block_count, block_len, number_of_heads, source.shape[-1])

    causal = jnp.tril(jnp.ones((block_len, block_len), jnp.float32))[:, :, None, None]

    def block_step(carry_state, inputs):
        query_blk, decay_blk, inflow_blk, value_blk = inputs
        cumulative = jnp.cumsum(decay_blk, axis=0)
        relative = cumulative[:, None] - cumulative[None, :]
        decay_table = jnp.exp(jnp.minimum(relative, 0.0)) * causal
        scores = jnp.einsum("thd,shd,tshd->hts", query_blk, inflow_blk, decay_table)
        block_out = jnp.einsum("hts,shv->thv", scores, value_blk)
        block_out = block_out + jnp.einsum(
            "thd,hdv->thv", query_blk * jnp.exp(cumulative), carry_state
        )
        last_log = cumulative[-1]
        new_state = jnp.exp(last_log)[:, :, None] * carry_state + jnp.einsum(
            "shd,shv->hdv", inflow_blk * jnp.exp(last_log[None] - cumulative), value_blk
        )
        return (new_state, block_out)

    zero_state = jnp.zeros((number_of_heads, key_width, value_rows.shape[-1]), jnp.float32)
    final_state, outputs = lax.scan(
        block_step,
        zero_state,
        (
            to_blocks(queries),
            to_blocks(decay_logarithm),
            to_blocks(state_inflow),
            to_blocks(value_rows),
        ),
    )
    return (final_state, outputs.reshape(token_count, number_of_heads, -1))


def chain_pair(earlier, following):
    return (earlier[0] * following[0], following[0][:, :, None] * earlier[1] + following[1])


def recurrent_path_output(
    recurrent_query,
    recurrent_forget_gate,
    recurrent_value,
    recurrent_gate_lower_bound,
    recurrent_added_decay,
    recurrent_norm_gain,
):
    token_count = recurrent_query.shape[0]
    number_of_heads = recurrent_gate_lower_bound.shape[0] // HG_DK
    state_inflow, decay_logarithm = decay_factors(
        recurrent_forget_gate, recurrent_gate_lower_bound, recurrent_added_decay, number_of_heads
    )
    queries = recurrent_query.astype(jnp.float32).reshape(token_count, number_of_heads, HG_DK)
    value_rows = recurrent_value.astype(jnp.float32).reshape(token_count, number_of_heads, HG_DV)
    final_state, local_out = recurrence_blocks(
        queries, decay_logarithm, state_inflow, value_rows, BLK
    )
    running_log = jnp.cumsum(decay_logarithm, axis=0)
    through = jnp.exp(running_log[-1])
    incoming = carried_in(
        (through, final_state),
        "sp",
        chain_pair,
        (jnp.ones_like(through), jnp.zeros_like(final_state)),
    )
    carried = jnp.einsum("thd,hdv->thv", queries * jnp.exp(running_log), incoming[1])
    return (
        head_norm(local_out + carried, recurrent_norm_gain)
        .astype(jnp.bfloat16)
        .reshape(token_count, -1)
    )


def attention_branch(
    attention_query_first,
    attention_key_first,
    attention_query_second,
    attention_key_second,
    attention_value,
    second_map_weight,
    attention_norm_gain,
):
    query_rows = attention_query_first.shape[0]
    key_heads = attention_key_first.shape[1] // DA_HD
    group_size = attention_query_first.shape[1] // DA_HD // key_heads
    score_scale = DA_HD ** (-0.5)
    offset = lax.axis_index("sp") * query_rows
    query_pos = offset + jnp.arange(query_rows)
    last_query = offset + query_rows - 1
    queries_one = attention_query_first.reshape(query_rows, key_heads, group_size, DA_HD)
    queries_two = attention_query_second.reshape(query_rows, key_heads, group_size, DA_HD)

    def map_update(running, queries, key_rows, value_rows, allowed):
        row_max, weight_mass, value_sum = running
        scores = (
            jnp.einsum("qkgd,skd->kgqs", queries, key_rows, preferred_element_type=jnp.float32)
            * score_scale
        )
        scores = jnp.where(allowed, scores, -1e30)
        new_max = jnp.maximum(row_max, jnp.max(scores, axis=-1))
        weights = jnp.where(allowed, jnp.exp(scores - new_max[..., None]), 0.0)
        shrink = jnp.exp(row_max - new_max)
        weight_mass = weight_mass * shrink + jnp.sum(weights, axis=-1)
        value_sum = value_sum * shrink[..., None] + jnp.einsum(
            "plew,wpd->pled",
            weights.astype(jnp.bfloat16),
            value_rows,
            preferred_element_type=jnp.float32,
        )
        return (new_max, weight_mass, value_sum)

    def key_block(running, block_one, block_two, block_values, first_row):
        span_rows = block_one.shape[0]
        key_pos = first_row + jnp.arange(span_rows)
        allowed = key_pos[None, :] <= query_pos[:, None]
        shaped_one = block_one.reshape(span_rows, key_heads, DA_HD)
        shaped_two = block_two.reshape(span_rows, key_heads, DA_HD)
        shaped_values = block_values.reshape(span_rows, key_heads, 2 * DA_HD)
        return (
            map_update(running[0], queries_one, shaped_one, shaped_values, allowed),
            map_update(running[1], queries_two, shaped_two, shaped_values, allowed),
        )

    def guarded_block(running, block_one, block_two, block_values, first_row):

        def compute(state_in):
            return key_block(state_in, block_one, block_two, block_values, first_row)

        def unchanged(state_in):
            return state_in

        result = lax.cond(first_row > last_query, unchanged, compute, running)
        return result

    start_max = jnp.full((key_heads, group_size, query_rows), -1e30, jnp.float32)
    zero_mass = jnp.zeros((key_heads, group_size, query_rows), jnp.float32)
    zero_sum = jnp.zeros((key_heads, group_size, query_rows, 2 * DA_HD), jnp.float32)
    fresh_state = (start_max, zero_mass, zero_sum)
    running = (fresh_state, fresh_state)
    shard_one, shard_two, shard_values = in_one_piece(
        (attention_key_first, attention_key_second, attention_value), "sp", 0, 1
    )
    row_count = shard_one.shape[0]
    span_rows = min(row_count, key_span)
    full_count = row_count // span_rows

    def span_step(span_index, state_in):
        begin_row = span_index * span_rows
        return guarded_block(
            state_in,
            lax.dynamic_slice_in_dim(shard_one, begin_row, span_rows, 0),
            lax.dynamic_slice_in_dim(shard_two, begin_row, span_rows, 0),
            lax.dynamic_slice_in_dim(shard_values, begin_row, span_rows, 0),
            begin_row,
        )

    running = lax.fori_loop(0, full_count, span_step, running)
    first_map, second_map = running
    lambda_table = second_map_weight.reshape(key_heads, group_size)[:, :, None, None]
    combined = first_map[2] / first_map[1][..., None] - lambda_table * (
        second_map[2] / second_map[1][..., None]
    )
    combined = jnp.transpose(combined, (2, 0, 1, 3)).reshape(
        query_rows, key_heads * group_size, 2 * DA_HD
    )
    return head_norm(combined, attention_norm_gain).astype(jnp.bfloat16).reshape(query_rows, -1)


def shards(
    recurrent_query,
    recurrent_forget_gate,
    recurrent_value,
    recurrent_gate_lower_bound,
    recurrent_added_decay,
    recurrent_norm_gain,
    attention_query_first,
    attention_key_first,
    attention_query_second,
    attention_key_second,
    attention_value,
    second_map_weight,
    attention_norm_gain,
    output_weight,
):
    attended = attention_branch(
        attention_query_first,
        attention_key_first,
        attention_query_second,
        attention_key_second,
        attention_value,
        second_map_weight,
        attention_norm_gain,
    )
    recurrent_output = recurrent_path_output(
        recurrent_query,
        recurrent_forget_gate,
        recurrent_value,
        recurrent_gate_lower_bound,
        recurrent_added_decay,
        recurrent_norm_gain,
    )
    pieces = lax.all_gather(output_weight, "sp", axis=2, tiled=True)
    partial_terms = jnp.dot(
        recurrent_output, pieces[0], preferred_element_type=jnp.float32
    ) + jnp.dot(attended, pieces[1], preferred_element_type=jnp.float32)
    return summed_on_arrival(partial_terms.astype(jnp.bfloat16), "tp", 0).astype(jnp.bfloat16)


def solution(mesh):
    return jax.shard_map(
        shards,
        mesh=mesh,
        in_specs=(
            P(("grp", "sp"), "tp"),
            P(("grp", "sp"), "tp"),
            P(("grp", "sp"), "tp"),
            P("tp"),
            P(("grp", "sp"), "tp"),
            P(),
            P(("grp", "sp"), "tp"),
            P(("grp", "sp"), "tp"),
            P(("grp", "sp"), "tp"),
            P(("grp", "sp"), "tp"),
            P(("grp", "sp"), "tp"),
            P("tp"),
            P(),
            P(None, "tp", "sp"),
        ),
        out_specs=P(("grp", "sp", "tp"), None),
        check_vma=False,
    )
```

profile of v0, /device:TPU:2016, one launch (start us, length us, event | category | flops | bytes accessed | tf_op | source)
XLA Modules:
  0.0 664.5 jit_solution(9917278042523082611)
XLA Ops:
  11.3 21.9 %while.52 = (s32[]{:T(128)}, f32[2,128,128]{2,1,0:T(8,128)S(1)}, f32[8,32,2,128]{3,1,0,2:T(8,128)S(1)}, f32[8,32,2,128]{3,2,1,0:T(2,128)S(1)}, f32[8,32,2,128]{3...) while((s32[]{:T(128)}, f32[2,128,128]{2,1,0:T(8,128)S(1)}, ...), condition=%wide.region_2.3_spmd.clone, body=%wide.region_0.2_spmd.clone.sunk | while | flops 6725635 | bytes 3266684 | solution.py:100
  36.9 51.6 %all_gather.16 = bf16[64,2,128]{2,1,0:T(2,128)(2,1)S(1)} all-gather(bf16[1,2,128]{2,1,0:T(2,128)(2,1)S(1)} %fusion.67), channel_id=1, replica_groups=mesh['grp'=2,'sp'=64,'tp'=4] {'sp'}, dimensions={0}, use_global_device_ids=true | all-gather | bytes 33280 | tf_op jit(solution)/shard_map/all_gather | solution.py:19
  89.2 64.9 %all-gather.9.cloned.1.call-done = bf16[128,128,128]{2,1,0:T(8,128)(2,1)} async-done(((bf16[2,128,128]{2,1,0:T(8,128)(2,1)}), bf16[128,128,128]{2,1,0:T(8,128)(2,1)}) %all-gather.9.cloned.1.call-update) | async-done | bytes 4194320 | tf_op jit(solution)/shard_map/all_gather | solution.py:19
  154.1 64.9 %while.53 = (s32[]{:T(128)}, f32[2,128,128]{2,1,0:T(8,128)S(1)}, s32[]{:T(128)}, bf16[64,2,128]{2,1,0:T(2,128)(2,1)S(1)}, bf16[64,2,128,128]{3,2,1,0:T(8,128)(2,1)}, /*index=5*/s32[]{:T(128)}, s32[]{:T(128)}) while((s32[]{:T(128)}, f32[2,128,128]{2,1,0:T(8,128)S(1)}, s32[]{:T(128)}, bf16[64,2,128]{2,1,0:T(2,128)(2,1)S(1)}, ...), condition=%wide.region_6.0_spmd.clone, body=%wide.region_5.6_spmd.clone.sunk | while | flops 164100 | bytes 330345 | solution.py:36
  219.4 63.2 %all-gather.5.cloned.1.call-done = bf16[2,256,2048]{1,2,0:T(8,128)(2,1)} async-done(((bf16[2,256,32]{1,2,0:T(8,128)(2,1)}), bf16[2,256,2048]{1,2,0:T(8,128)(2,1)}) %all-gather.5.cloned.1.call-update) | async-done | bytes 2097168 | tf_op jit(solution)/shard_map/all_gather | solution.py:279
  284.2 148.2 %all-gather.7.cloned.1.call-done = bf16[16384,256]{0,1:T(8,128)(2,1)} async-done(((bf16[256,256]{0,1:T(8,128)(2,1)}), bf16[16384,256]{0,1:T(8,128)(2,1)}) %all-gather.7.cloned.1.call-update) | async-done | bytes 8388624 | tf_op jit(solution)/shard_map/all_gather | solution.py:45
  436.9 6.3 copy.178
  447.9 187.3 %while.51 = (s32[]{:T(128)}, f32[1,2,256]{2,1,0:T(2,128)S(1)}, f32[1,2,256]{2,1,0:T(2,128)S(1)}, f32[1,2,256,128]{3,2,1,0:T(8,128)S(1)}, f32[1,2,256]{2,1,0:T(2,...) while((s32[]{:T(128)}, f32[1,2,256]{2,1,0:T(2,128)S(1)}, ...), condition=%wide.region_15.16_spmd.clone, body=%wide.region_8.15_spmd.clone.sunk | while | flops 206442240 | bytes 8724921 | solution.py:234
  448.0 5.8 conditional.3
  453.8 5.8 conditional.3
  459.7 5.8 conditional.3
  465.5 5.8 conditional.3
  471.4 5.8 conditional.3
  477.2 5.8 conditional.3
  483.1 5.8 conditional.3
  488.9 5.8 conditional.3
  494.8 5.8 conditional.3
  500.6 5.8 conditional.3
  506.5 5.8 conditional.3
  512.3 5.8 conditional.3
  518.2 5.8 conditional.3
  524.1 5.8 conditional.3
  529.9 5.8 conditional.3
  535.8 5.8 conditional.3
  541.6 5.8 conditional.3
  547.5 5.8 conditional.3
  553.3 5.8 conditional.3
  559.2 5.8 conditional.3
  565.0 5.8 conditional.3
  570.9 5.8 conditional.3
  576.7 5.8 conditional.3
  637.5 19.5 %all_to_all.5 = bf16[4,64,2048]{2,1,0:T(8,128)(2,1)S(1)} all-to-all(bf16[4,64,2048]{2,1,0:T(8,128)(2,1)S(1)} %bitcast.200), channel_id=1, replica_groups=mesh['grp'=2,'sp'=64,'tp'=4] {'tp'}, dimensions={0} | all-to-all | bytes 2097152 | tf_op jit(solution)/shard_map/all_to_all | solution.py:55
  (775 shorter events, 341.9 us)
Async XLA Ops:
  6.5 4.2 copy-start
  6.5 147.6 %all-gather.9.cloned.1.call-start = ((), (), s32[]{:S(2)}) async-start(), calls=%async_computation.3 | async-start | bytes 4259840 | tf_op jit(solution)/shard_map/all_gather | solution.py:19
  11.3 23.5 %copy-start.1 = (bf16[256,128]{1,0:T(8,128)(2,1)S(1)}, bf16[256,128]{1,0:T(8,128)(2,1)}, u32[]{:S(2)}) copy-start(bf16[256,128]{1,0:T(8,128)(2,1)} %param.32) | copy-start | bytes 196612
  11.3 23.7 %copy-start.4 = (bf16[256,64]{0,1:T(8,128)(2,1)S(1)}, bf16[256,64]{0,1:T(8,128)(2,1)}, u32[]{:S(2)}) copy-start(bf16[256,64]{0,1:T(8,128)(2,1)} %param.31) | copy-start | bytes 98308
  11.3 23.7 %copy-start.5 = (bf16[256,64]{0,1:T(8,128)(2,1)S(1)}, bf16[256,64]{0,1:T(8,128)(2,1)}, u32[]{:S(2)}) copy-start(bf16[256,64]{0,1:T(8,128)(2,1)} %param.29) | copy-start | bytes 98308
  11.3 24.4 %copy-start.2 = (bf16[256,128]{1,0:T(8,128)(2,1)S(1)}, bf16[256,128]{1,0:T(8,128)(2,1)}, u32[]{:S(2)}) copy-start(bf16[256,128]{1,0:T(8,128)(2,1)} %param.28) | copy-start | bytes 196612
  11.3 24.5 %copy-start.3 = (bf16[256,128]{1,0:T(8,128)(2,1)S(1)}, bf16[256,128]{1,0:T(8,128)(2,1)}, u32[]{:S(2)}) copy-start(bf16[256,128]{1,0:T(8,128)(2,1)} %param.30) | copy-start | bytes 196612
  11.3 24.7 %copy-start.6 = (f32[256,2]{0,1:T(2,128)S(1)}, f32[256,2]{0,1:T(2,128)}, u32[]{:S(2)}) copy-start(f32[256,2]{0,1:T(2,128)} %param.26) | copy-start | bytes 6148
  33.9 248.6 %all-gather.5.cloned.1.call-start = ((), (), s32[]{:S(2)}) async-start(), calls=%async_computation.1 | async-start | bytes 2129920 | tf_op jit(solution)/shard_map/all_gather | solution.py:279
  34.7 397.7 %all-gather.7.cloned.1.call-start = ((), (), s32[]{:S(2)}) async-start(), calls=%async_computation.2 | async-start | bytes 8519680 | tf_op jit(solution)/shard_map/all_gather | solution.py:45
  88.6 130.7 %copy-start.7 = (f32[128]{0:T(128)S(1)}, f32[128]{0:T(128)}, u32[]{:S(2)}) copy-start(f32[128]{0:T(128)} %param.27) | copy-start | bytes 1540
  447.9 187.6 %copy-start.9 = (f32[2]{0:T(128)S(1)}, f32[2]{0:T(128)}, u32[]{:S(2)}) copy-start(f32[2]{0:T(128)} %param.33) | copy-start | bytes 28
  447.9 187.7 %copy-start.8 = (f32[128]{0:T(128)S(1)}, f32[128]{0:T(128)}, u32[]{:S(2)}) copy-start(f32[128]{0:T(128)} %param.34) | copy-start | bytes 1540
Sparse Core Ops, SparseCore 0:
  34.0 120.0 all-gather.8
  156.3 126.2 all-gather.4
  284.6 147.8 all-gather.6
where the time goes:
time: 672 us; the launch traced here: 664 us
  waiting for transfers between devices  277 us (41%)
  matrix products  172 us (26%)
  other arithmetic  102 us (15%)
  blocking collectives  71.2 us (11%)
  local copies, waits for them, and re-layouts  20.7 us (3%)
  between operations  13.6 us (2%)
  loops' own time  7.26 us (1%)
    all_gather x1, waiting for transfers between devices, in_one_piece(): lax.all_gather(both, axis, axis=dim, tiled=True)  148 us
    dot_general x64, matrix products, map_update(): jnp.einsum('plew,wpd->pled', weights.astype(jnp.bfloat16), value_rows, pr...  88.7 us
    dot_general x64, matrix products, map_update(): jnp.einsum('qkgd,skd->kgqs', queries, key_rows, preferred_element_type=jn...  75.2 us
    all_gather x1, waiting for transfers between devices, carried_in(): lax.all_gather(part.astype(kind), axis)  64.9 us
    all_gather x1, waiting for transfers between devices, shards(): pieces = lax.all_gather(output_weight, 'sp', axis=2, tiled=True)  63.2 us
    select_n x64, other arithmetic, hop(): return jax.tree.map(lambda a, b: jnp.where(reached, a, b), new, before)  62.1 us
    all_gather x1, blocking collectives, carried_in(): lax.all_gather(part.astype(kind), axis)  51.6 us
    all_to_all x1, blocking collectives, summed_on_arrival(): pieces = lax.all_to_all(split_up(array, dim, size), axis, 0, 0, tiled=True)  19.5 us
  transfers between devices with their start and end apart: 3, of which 3 were waited for; matrix products, arithmetic and copies ran while one was open for 10% of the time, Pallas kernels for 0%

commit v1 on v0

v1 whole, which is shorter than its diff:
```python
import functools

import jax
import jax.numpy as jnp
from jax import lax
from jax.experimental import pallas as pl
from jax.experimental.pallas import tpu as pltpu
from jax.sharding import PartitionSpec as P

HEAD = 128
DA_HD = 64
BLK = 64
HOPS = 4
EPS = 1e-06
f32, bf16 = jnp.float32, jnp.bfloat16
NT = (((1,), (1,)), ((), ()))
TN = (((0,), (0,)), ((), ()))


def dot(a, b, dims=(((1,), (0,)), ((), ())), precision=None):
    return lax.dot_general(a, b, dims, precision=precision, preferred_element_type=f32)


def kernel(
    nz, kvl, wl, qp, rq, fg, rv, lb, added, lam, rgain, again, out,
    kv, wbuf, acc, mrow, sown, spart, tm, ch, pe, loc, qe, dev_state, dev_decay,
    arec, aatt, ract, part,
    copy_sem, send_sem, kvz_sem, kvp_sem, wz_sem, wx_sem, wr_sem, wp_sem, st_sem, act_sem,
):
    g, sp, x = lax.axis_index("grp"), lax.axis_index("sp"), lax.axis_index("tp")
    ntp = lax.axis_size("tp")
    z, c = sp // 2, sp % 2
    half = nz // 2
    kv_reach = (half - 1, half)
    w_reach = (half, half - 1)
    tok = rq.shape[0]
    rows_out = tok // ntp

    def zdev(dz):
        return (g, ((z + dz + nz) % nz) * 2 + c, x)

    def xdev(dx):
        return (g, sp, (x + dx + ntp) % ntp)

    partner = (g, z * 2 + 1 - c, x)
    ring = (zdev(1), zdev(-1))

    def send(src, dst, s_sem, r_sem, to):
        pltpu.make_async_remote_copy(
            src_ref=src, dst_ref=dst, send_sem=s_sem, recv_sem=r_sem,
            device_id=to, device_id_type=pl.DeviceIdType.MESH,
        ).start()

    def got(ref, sem):
        pltpu.make_async_copy(ref, ref, sem).wait()

    def chip_at(d, i):
        return (z - i + nz) % nz if d == 0 else (z + i) % nz

    cp_kv = pltpu.make_async_copy(kvl, kv.at[sp], copy_sem.at[0])
    cp_w = pltpu.make_async_copy(wl, wbuf.at[0, sp], copy_sem.at[1])
    cp_kv.start()
    cp_w.start()
    tm[...] = jnp.zeros_like(tm)
    ch[...] = jnp.zeros_like(ch)

    barrier = pltpu.get_barrier_semaphore()
    near = [zdev(1), zdev(-1), zdev(HOPS), zdev(-HOPS), xdev(1), xdev(2), xdev(3), partner]
    for dev in near:
        pl.semaphore_signal(barrier, inc=1, device_id=dev, device_id_type=pl.DeviceIdType.MESH)
    pl.semaphore_wait(barrier, len(near))

    s_kvz, s_kvp, s_wz, s_wx, s_wr, s_wp, s_act, s_own, s_chain, s_pe = (
        send_sem.at[k] for k in range(10)
    )
    s_tm = [send_sem.at[10 + r] for r in range(HOPS)]

    cp_kv.wait()
    for kind in range(2):
        mine = kv.at[sp, kind]
        send(mine, mine, s_kvz, kvz_sem.at[0, kind], ring[0])
        send(mine, mine, s_kvz, kvz_sem.at[1, kind], ring[1])
    for kind in range(2):
        mine = kv.at[sp, kind]
        send(mine, mine, s_kvp, kvp_sem.at[0, 2 * half + kind], partner)
    cp_w.wait()
    mine = wbuf.at[0, sp]
    send(mine, mine, s_wz, wz_sem.at[0, 1], ring[0])
    send(mine, mine, s_wz, wz_sem.at[1, 1], ring[1])
    send(mine, wbuf.at[3, sp], s_wx, wx_sem.at[1, 0, 0], xdev(1))
    send(mine, wbuf.at[1, sp], s_wx, wx_sem.at[0, 0, 0], xdev(-1))
    send(mine, mine, s_wp, wp_sem.at[0], partner)

    floor_rate = jax.nn.sigmoid(-lb[...])
    inflow = floor_rate * jax.nn.sigmoid(-fg[...].astype(f32))
    one_less = 1.0 - inflow
    add2 = added[...]
    add_wide = jnp.concatenate(
        [jnp.broadcast_to(add2[:, h : h + 1], (tok, HEAD)) for h in range(2)], axis=1
    )
    log_decay = jnp.log(one_less) - ((one_less - 1.0) + inflow) / one_less + add_wide
    row = lax.broadcasted_iota(jnp.int32, (tok, tok), 0)
    col = lax.broadcasted_iota(jnp.int32, (tok, tok), 1)
    tri = jnp.where(col <= row, 1.0, 0.0).astype(f32)
    cum = dot(tri, log_decay, precision=lax.Precision.HIGHEST)
    last = cum[tok - 1 : tok, :]
    kin = (inflow * jnp.exp(last - cum)).astype(bf16)
    through = jnp.exp(last)
    r16 = lax.broadcasted_iota(jnp.int32, (16, HEAD), 0)

    def pack_decay(dec):
        hi = dec.astype(bf16)
        lo = (dec - hi.astype(f32)).astype(bf16)
        zero = jnp.zeros((16, HEAD), f32)
        return jnp.where(
            r16 == 0, hi.astype(f32), jnp.where(r16 == 1, lo.astype(f32), zero)
        ).astype(bf16)

    def unpack_decay(msg):
        rows = msg[HEAD : HEAD + 16, :].astype(f32)
        return rows[0:1] + rows[1:2]

    def unpack_state(msg):
        return msg[0:HEAD, :].astype(f32)

    for h in range(2):
        cols = slice(h * HEAD, (h + 1) * HEAD)
        st = dot(rv[:, cols], kin[:, cols], TN)
        dev_state[h] = st
        dev_decay[h] = through[:, cols]
        sown[h, 0:HEAD, :] = st.astype(bf16)
        sown[h, HEAD : HEAD + 16, :] = pack_decay(through[:, cols])
    send(sown, spart, s_own, st_sem.at[0], partner)
    qe[...] = (rq[...].astype(f32) * jnp.exp(cum)).astype(bf16)

    def local_outputs():
        r64 = lax.broadcasted_iota(jnp.int32, (BLK, BLK), 0)
        c64 = lax.broadcasted_iota(jnp.int32, (BLK, BLK), 1)
        for h in range(2):
            cols = slice(h * HEAD, (h + 1) * HEAD)
            state = None
            for b in range(tok // BLK):
                rows = slice(b * BLK, (b + 1) * BLK)
                blk_cum = cum[rows, cols]
                if b:
                    blk_cum = blk_cum - cum[b * BLK - 1 : b * BLK, cols]
                qd = (rq[rows, cols].astype(f32) * jnp.exp(blk_cum)).astype(bf16)
                kd = (inflow[rows, cols] * jnp.exp(-blk_cum)).astype(bf16)
                scores = dot(qd, kd, NT)
                scores = jnp.where(c64 <= r64, scores, 0.0).astype(bf16)
                res = dot(scores, rv[rows, cols])
                if b:
                    res = res + dot(qd, state.astype(bf16), NT)
                loc[rows, cols] = res
                if b + 1 < tok // BLK:
                    end = blk_cum[BLK - 1 : BLK, :]
                    ke = (inflow[rows, cols] * jnp.exp(end - blk_cum)).astype(bf16)
                    new = dot(rv[rows, cols], ke, TN)
                    state = new if b == 0 else state * jnp.exp(end) + new

    local_outputs()

    got(spart, st_sem.at[0])
    own_s, own_d = dev_state[c], dev_decay[c]
    oth_s, oth_d = unpack_state(spart[c]), unpack_decay(spart[c])
    first_core = c == 0
    late_d = jnp.where(first_core, oth_d, own_d)
    chip_state = late_d * jnp.where(first_core, own_s, oth_s) + jnp.where(first_core, oth_s, own_s)
    tm[0, 0:HEAD, :] = chip_state.astype(bf16)
    tm[0, HEAD : HEAD + 16, :] = pack_decay(own_d * oth_d)

    @pl.when(z + 1 < nz)
    def _():
        send(tm.at[0], tm.at[1], s_tm[0], st_sem.at[1], zdev(1))

    ones = jnp.ones((16, 2 * tok), bf16)

    def pair_update(chip, fresh):
        s0 = chip * 2
        keys = jnp.concatenate([kv[s0, 0], kv[s0 + 1, 0]], axis=0)
        vt = jnp.concatenate(
            [
                kv[s0, 1, 0:HEAD, :], kv[s0, 1, HEAD : 2 * HEAD, :],
                kv[s0 + 1, 1, 0:HEAD, :], kv[s0 + 1, 1, HEAD : 2 * HEAD, :],
            ],
            axis=1,
        )
        vt = jnp.concatenate([vt, ones], axis=0)
        for t in range(4):
            s = dot(keys, qp[t], NT)
            if fresh:
                kpos = lax.broadcasted_iota(jnp.int32, s.shape, 0)
                qpos = lax.broadcasted_iota(jnp.int32, s.shape, 1) + c * tok
                s = jnp.where(kpos <= qpos, s, -1e30)
                new_max = jnp.max(s, axis=0, keepdims=True)
                w = jnp.where(kpos <= qpos, jnp.exp(s - new_max), 0.0).astype(bf16)
                acc[t] = dot(vt, w)
            else:
                old_max = mrow[t]
                new_max = jnp.maximum(old_max, jnp.max(s, axis=0, keepdims=True))
                w = jnp.exp(s - new_max).astype(bf16)
                acc[t] = acc[t] * jnp.exp(old_max - new_max) + dot(vt, w)
            mrow[t] = new_max

    def take_pair(d, i):
        chip = chip_at(d, i)
        slot = chip * 2 + 1 - c
        for kind in range(2):
            got(kv.at[slot, kind], kvp_sem.at[d, 2 * (i - 1) + kind])
        earlier = (z >= i) if d == 0 else (z + i >= nz)

        @pl.when(earlier)
        def _():
            pair_update(chip, False)

    def forward_kv(p):
        i, kind = p // 2 + 1, p % 2
        for d in range(2):

            @pl.when(i <= kv_reach[d])
            def _():
                piece = kv.at[chip_at(d, i) * 2 + c, kind]
                got(piece, kvz_sem.at[d, p])

                @pl.when(i < kv_reach[d])
                def _():
                    send(piece, piece, s_kvz, kvz_sem.at[d, p + 2], ring[d])

                send(piece, piece, s_kvp, kvp_sem.at[d, p], partner)

    def forward_w(p):
        i = p + 1
        for d in range(2):

            @pl.when(i <= w_reach[d])
            def _():
                s = chip_at(d, i) * 2 + c
                piece = wbuf.at[0, s]
                got(piece, wz_sem.at[d, i])

                @pl.when(i < w_reach[d])
                def _():
                    send(piece, piece, s_wz, wz_sem.at[d, i + 1], ring[d])

                send(piece, wbuf.at[3, s], s_wx, wx_sem.at[1, d, i], xdev(1))
                send(piece, wbuf.at[1, s], s_wx, wx_sem.at[0, d, i], xdev(-1))
                send(piece, piece, s_wp, wp_sem.at[0], partner)

        j = p - 1
        for d in range(2):

            @pl.when((j >= d) & (j <= w_reach[d]))
            def _():
                s = chip_at(d, j) * 2 + c
                for k in range(2):
                    rel = 2 * k + 1
                    got(wbuf.at[rel, s], wx_sem.at[k, d, j])
                    send(wbuf.at[rel, s], wbuf.at[rel, s], s_wp, wp_sem.at[0], partner)
                send(wbuf.at[3 - 2 * c, s], wbuf.at[2, s], s_wr, wr_sem.at[d, j], xdev(1 - 2 * c))

        k = p - 3
        for d in range(2):

            @pl.when((k >= d) & (k <= w_reach[d]))
            def _():
                s = chip_at(d, k) * 2 + c
                got(wbuf.at[2, s], wr_sem.at[d, k])
                send(wbuf.at[2, s], wbuf.at[2, s], s_wp, wp_sem.at[0], partner)

    def hand_out(src, which):
        for r in range(1, 4):
            d = (x - r + ntp) % ntp
            rows = src.at[pl.ds(pl.multiple_of(d * rows_out, rows_out), rows_out)]
            send(rows, ract.at[which, r], s_act, act_sem.at[which, r], (g, sp, d))

    turn = 2 * HOPS + 3 * (z // HOPS)

    def state_steps(p):
        @pl.when((p % 2 == 0) & (p >= 2) & (p <= 2 * HOPS))
        def _():
            r = p // 2

            @pl.when(z >= r)
            def _():
                got(tm.at[r], st_sem.at[r])

                @pl.when((r < HOPS) & (z + 1 < nz))
                def _():
                    send(tm.at[r], tm.at[r + 1], send_sem.at[10 + r], st_sem.at[r + 1], zdev(1))

        @pl.when(p == turn)
        def _():
            @pl.when(z >= HOPS)
            def _():
                got(ch.at[0], st_sem.at[HOPS + 1])

            state = unpack_state(ch[0])
            for r in range(HOPS, 0, -1):
                state = state * unpack_decay(tm[r]) + unpack_state(tm[r])
            ch[1, 0:HEAD, :] = state.astype(bf16)

            @pl.when(z + HOPS < nz)
            def _():
                send(ch.at[1], ch.at[0], s_chain, st_sem.at[HOPS + 1], zdev(HOPS))

            send(ch.at[1], pe, s_pe, st_sem.at[HOPS + 2], partner)

        @pl.when(p == turn + 1)
        def _():
            got(pe, st_sem.at[HOPS + 2])
            ours, theirs = unpack_state(ch[1]), unpack_state(pe[...])
            for h in range(2):
                cols = slice(h * HEAD, (h + 1) * HEAD)
                before = jnp.where(c == h, ours, theirs)
                second = before * unpack_decay(spart[h]) + unpack_state(spart[h])
                before = jnp.where(first_core, before, second).astype(bf16)
                mix = loc[:, cols] + dot(qe[:, cols], before, NT)
                mean_square = jnp.mean(mix * mix, axis=-1, keepdims=True)
                arec[:, cols] = (mix * lax.rsqrt(mean_square + EPS) * rgain[...]).astype(bf16)
            hand_out(arec, 0)

    def phase(p, carry):
        forward_kv(p)
        forward_w(p)
        state_steps(p)

        @pl.when(p == 0)
        def _():
            for kind in range(2):
                got(kv.at[z * 2 + 1 - c, kind], kvp_sem.at[0, 2 * half + kind])
            pair_update(z, True)

        i = p // 2
        for d in range(2):

            @pl.when((p >= 2) & (p % 2 == d) & (i <= kv_reach[d]))
            def _():
                take_pair(d, i)

        return carry

    lax.fori_loop(0, 2 * half, phase, 0)
    take_pair(1, half)

    for h in range(2):
        cols = slice(h * HEAD, (h + 1) * HEAD)
        one, two = acc[h], acc[2 + h]
        mix = one[0:HEAD] / one[HEAD : HEAD + 1]
        mix = mix - lam[h : h + 1, 0:1] * (two[0:HEAD] / two[HEAD : HEAD + 1])
        mean_square = jnp.mean(mix * mix, axis=0, keepdims=True)
        mix = jnp.transpose(mix * lax.rsqrt(mean_square + EPS))
        aatt[:, cols] = (mix * again[...]).astype(bf16)
    hand_out(aatt, 1)

    got(wbuf.at[0:4, 0:nz], wp_sem.at[0])
    chunk = 512
    pieces = chunk // 32

    def project(which, src):
        own_rows = src[pl.ds(pl.multiple_of(x * rows_out, rows_out), rows_out), :]
        acts = [own_rows if r == 0 else ract[which, r] for r in range(4)]

        def columns(n):
            total = None
            for r in range(4):
                w = [
                    wbuf[
                        r, pl.ds(n * pieces, pieces),
                        which * 64 + kb * 32 : which * 64 + kb * 32 + 32, :
                    ].reshape(chunk, HEAD)
                    for kb in range(2)
                ]
                term = dot(acts[r], jnp.concatenate(w, axis=1), NT)
                total = term if total is None else total + term
            return total

        return columns

    for r in range(1, 4):
        got(ract.at[0, r], act_sem.at[0, r])
    rec = project(0, arec)
    for n in range(2048 // chunk):
        part[:, n * chunk : (n + 1) * chunk] = rec(n)
    for r in range(1, 4):
        got(ract.at[1, r], act_sem.at[1, r])
    att = project(1, aatt)
    for n in range(2048 // chunk):
        cols = slice(n * chunk, (n + 1) * chunk)
        out[:, cols] = (part[:, cols] + att(n)).astype(bf16)

    got(kv.at[0 : nz - 1], s_kvz)
    got(kv.at[0:nz], s_kvp)
    got(wbuf.at[0, 0 : nz - 1], s_wz)
    got(wbuf.at[0:2, 0:nz], s_wx)
    got(wbuf.at[0, 0:nz], s_wr)
    got(wbuf.at[0:4, 0:nz], s_wp)
    got(sown, s_own)
    got(pe, s_pe)

    @pl.when(z + HOPS < nz)
    def _():
        got(pe, s_chain)

    for r in range(HOPS):

        @pl.when((z + 1 < nz) & (z >= r))
        def _():
            got(pe, s_tm[r])

    got(ract.at[0:2, 1:4], s_act)


def shards(rq, fg, rv, lb, added, rgain, q1, k1, q2, k2, v, lam, again, w, *, nz):
    tok = rq.shape[0]
    half_tok = tok // 2
    keys = jnp.concatenate([k1, k2], axis=1)
    vt = v.reshape(2, half_tok, HEAD).transpose(0, 2, 1).reshape(tok, HEAD)
    kvl = jnp.stack([keys, vt])
    wl = w.reshape(2, 2, HEAD, 32).transpose(0, 1, 3, 2).reshape(HEAD, HEAD)
    scale = jnp.asarray(DA_HD**-0.5, bf16)
    zero = jnp.zeros((tok, DA_HD), bf16)
    qp = jnp.stack(
        [
            jnp.concatenate([q1[:, :DA_HD] * scale, zero], axis=1),
            jnp.concatenate([q1[:, DA_HD:] * scale, zero], axis=1),
            jnp.concatenate([zero, q2[:, :DA_HD] * scale], axis=1),
            jnp.concatenate([zero, q2[:, DA_HD:] * scale], axis=1),
        ]
    )
    vmem = pl.BlockSpec(memory_space=pltpu.VMEM)
    hbm = pl.BlockSpec(memory_space=pltpu.HBM)
    nsp = 2 * nz
    msg = (HEAD + 16, HEAD)
    dma = pltpu.SemaphoreType.DMA
    return pl.pallas_call(
        functools.partial(kernel, nz),
        out_shape=jax.ShapeDtypeStruct((tok // 4, w.shape[2] * nsp), bf16),
        in_specs=[hbm, hbm] + [vmem] * 9,
        out_specs=vmem,
        scratch_shapes=[
            pltpu.VMEM((nsp, 2, tok, HEAD), bf16),
            pltpu.VMEM((4, nsp, HEAD, HEAD), bf16),
            pltpu.VMEM((4, HEAD + 16, tok), f32),
            pltpu.VMEM((4, 1, tok), f32),
            pltpu.VMEM((2,) + msg, bf16),
            pltpu.VMEM((2,) + msg, bf16),
            pltpu.VMEM((HOPS + 1,) + msg, bf16),
            pltpu.VMEM((2,) + msg, bf16),
            pltpu.VMEM(msg, bf16),
            pltpu.VMEM((tok, 2 * HEAD), f32),
            pltpu.VMEM((tok, 2 * HEAD), bf16),
            pltpu.VMEM((2, HEAD, HEAD), f32),
            pltpu.VMEM((2, 1, HEAD), f32),
            pltpu.VMEM((tok, 2 * HEAD), bf16),
            pltpu.VMEM((tok, 2 * HEAD), bf16),
            pltpu.VMEM((2, 4, tok // 4, 2 * HEAD), bf16),
            pltpu.VMEM((tok // 4, w.shape[2] * nsp), f32),
            dma((2,)),
            dma((10 + HOPS,)),
            dma((2, nz + 2)),
            dma((2, nz + 2)),
            dma((2, nz // 2 + 1)),
            dma((2, 2, nz // 2 + 1)),
            dma((2, nz // 2 + 1)),
            dma((1,)),
            dma((HOPS + 3,)),
            dma((2, 4)),
        ],
        compiler_params=pltpu.CompilerParams(
            collective_id=0, has_side_effects=True, vmem_limit_bytes=60 * 1024 * 1024
        ),
    )(
        kvl, wl, qp, rq, fg, rv, lb.reshape(1, -1), added,
        jnp.broadcast_to(lam[:, None], (2, HEAD)), rgain.reshape(1, -1), again.reshape(1, -1),
    )


def solution(mesh):
    tokens = P(("grp", "sp"), "tp")
    return jax.shard_map(
        functools.partial(shards, nz=mesh.shape["sp"] // 2),
        mesh=mesh,
        in_specs=(
            tokens, tokens, tokens, P("tp"), tokens, P(),
            tokens, tokens, tokens, tokens, tokens, P("tp"), P(), P(None, "tp", "sp"),
        ),
        out_specs=P(("grp", "sp", "tp"), None),
        check_vma=False,
    )
```

time: 672 us -> 155 us (0.23)
  the two profiles are of different devices: /device:TPU:2016 before, /device:TPU:33 now
where the time goes in v1:
time: 155 us
  Pallas kernels  146 us (94%)
  local copies, waits for them, and re-layouts  7.25 us (5%)
  other arithmetic  1.68 us (1%)
    pallas_call x1, Pallas kernels, shards(): pl.pallas_call(functools.partial(kernel, nz), out_shape=jax.ShapeDtypeStr...  146 us
    unnamed x20, local copies, waits for them, and re-layouts  5.75 us

profile of v1, /device:TPU:33, one launch (start us, length us, event | category | flops | bytes accessed | tf_op | source)
XLA Modules:
  0.0 154.5 jit_solution(6443983942404574582)
XLA Ops:
  0.0 0.0 copy-start
  0.0 0.0 copy-start.7
  0.0 0.7 copy-done.7
  0.7 0.6 broadcast_in_dim.2.lam
  1.3 0.0 copy-done
  1.3 0.0 copy-start.4
  1.3 0.6 copy_bitcast_fusion
  1.9 0.2 copy-done.4
  2.1 0.0 copy-start.5
  2.1 0.1 copy.15
  2.2 0.6 copy-done.5
  2.8 0.1 copy.16
  2.9 0.0 copy-start.3
  3.0 0.1 maximum_bitcast_fusion
  3.1 0.7 copy-done.3
  3.8 0.1 copy.17
  3.9 0.0 copy-start.6
  3.9 0.7 pad_maximum_fusion.1.kvl
  4.6 0.0 copy-done.6
  4.6 0.0 copy-start.1
  4.6 0.8 copy.19.added
  5.4 0.1 copy-done.1
  5.4 0.1 slice_multiply_fusion.3
  5.5 0.0 copy-start.2
  5.6 0.8 copy-done.2
  6.4 0.1 slice_multiply_fusion.1
  6.5 0.1 pad_bitcast_fusion
  6.6 0.7 pad_maximum_fusion.qp
  7.3 145.5 %shard_map.136 = bf16[64,2048]{1,0:T(8,128)(2,1)} custom-call(bf16[2,256,128]{2,1,0:T(8,128)(2,1)} %pad_maximum_fusion.1.kvl, bf16[128,128]{1,0:T(8,128)(2,1)} %bitcast.26, bf16[4,256,128]{2,1,0:T(8,128)(2,1)} %pad_maximum_fusion.qp, bf16[256,256]{1,0:T(8,128)(2,1)} %rq.1, bf16[256,256]{1,0:T(8,128)(2,1)} %fg.1, bf16[256,256]{1,0:T(8,128)(2,1)} %rv.1, ...), custom_call_target="tpu_custom_call" | custom-call | tf_op jit(solution)/shard_map/pallas_call | solution.py:435
  152.8 1.7 %copy.23 = bf16[64,2048]{1,0:T(8,128)(2,1)} copy(bf16[64,2048]{1,0:T(8,128)(2,1)} %shard_map.136) | data formatting | bytes 524288
  (1 shorter events, 0.0 us)
Async XLA Ops:
  0.0 1.3 copy-start
  0.0 0.7 copy-start.7
  1.3 0.8 copy-start.4
  2.1 0.8 copy-start.5
  2.9 0.8 copy-start.3
  3.9 0.7 copy-start.6
  4.6 0.8 copy-start.1
  5.5 0.8 copy-start.2

commit v2 on v1

v2 whole, which is shorter than its diff:
```python
import functools

import jax
import jax.numpy as jnp
from jax import lax
from jax.experimental import pallas as pl
from jax.experimental.pallas import tpu as pltpu
from jax.sharding import PartitionSpec as P

HEAD = 128
DA_HD = 64
BLK = 64
HOPS = 4
EPS = 1e-06
f32, bf16 = jnp.float32, jnp.bfloat16
NT = (((1,), (1,)), ((), ()))
TN = (((0,), (0,)), ((), ()))


def dot(a, b, dims=(((1,), (0,)), ((), ())), precision=None):
    return lax.dot_general(a, b, dims, precision=precision, preferred_element_type=f32)


def kernel(
    nz, kvl, wl, qp, rq, fg, rv, lb, added, lam, rgain, again, out,
    kv, wbuf, acc, mrow, sown, spart, tm, ch, pe, loc, qe, dev_state, dev_decay,
    arec, aatt, ract, part,
    copy_sem, send_sem, skz_sem, skp_sem, kvz_sem, kvp_sem, kvo_sem, wz_sem, wx_sem, wr_sem,
    wp_sem, st_sem, act_sem, chain_ready, wrap_ready,
):
    g, sp, x = lax.axis_index("grp"), lax.axis_index("sp"), lax.axis_index("tp")
    ntp = lax.axis_size("tp")
    z, c = sp // 2, sp % 2
    up = c == 0
    top = nz - 1
    half = nz // 2
    kv_up = (5 * nz) // 8
    kv_wrap = nz - 1 - kv_up
    w_far = (half, half - 1)
    gap = jnp.maximum(half // 2 + 1 - z, 0)
    meet = 10
    tok = rq.shape[0]
    rows_out = tok // ntp
    mesh_id = pl.DeviceIdType.MESH

    def zdev(chip):
        return (g, chip * 2 + c, x)

    def xdev(dx):
        return (g, sp, (x + dx + ntp) % ntp)

    partner = (g, z * 2 + 1 - c, x)
    ring = (zdev((z + 1) % nz), zdev((z - 1 + nz) % nz))

    def send(src, dst, s_sem, r_sem, to):
        pltpu.make_async_remote_copy(
            src_ref=src, dst_ref=dst, send_sem=s_sem, recv_sem=r_sem,
            device_id=to, device_id_type=mesh_id,
        ).start()

    def got(ref, sem):
        pltpu.make_async_copy(ref, ref, sem).wait()

    def tell(sem, dev):
        pl.semaphore_signal(sem, inc=1, device_id=dev, device_id_type=mesh_id)

    def chip_from(d, i):
        return (z - i + nz) % nz if d == 0 else (z + i) % nz

    def item(d, u):
        if d == 1:
            return u
        return jnp.where(u <= z, u, jnp.where(u > z + gap, u - gap, -1))

    def kv_used(d, i):
        if d == 0:
            return (i >= 1) & (i <= kv_up) & (z >= i)
        return (i >= 1) & (i <= kv_wrap) & (z + i >= nz)

    def kv_in(d, i):
        if d == 0:
            return kv_used(0, i)
        return kv_used(1, i) | (i >= 1) & (z + i < kv_wrap)

    def kv_out(d, i):
        own = z < (top if d == 0 else kv_wrap)
        on = (z < top) & (i < kv_up) if d == 0 else i < kv_wrap
        return (i == 0) & own | kv_in(d, i) & on

    def kv_pair(kind, chip):
        return kv.at[kind, pl.ds(2 * chip, 2)]

    loads = [pltpu.make_async_copy(kvl.at[k], kv.at[k, sp], copy_sem.at[k]) for k in range(2)]
    loads.append(pltpu.make_async_copy(wl, wbuf.at[0, sp], copy_sem.at[2]))
    for load in loads:
        load.start()
    tm[...] = jnp.zeros_like(tm)
    ch[...] = jnp.zeros_like(ch)

    barrier = pltpu.get_barrier_semaphore()

    def greet(cond, dev):
        @pl.when(cond)
        def _():
            tell(barrier, dev)

    for dx in range(1, 4):
        tell(barrier, xdev(dx))
    tell(barrier, partner)
    greet(z < top, zdev(jnp.minimum(z + 1, top)))
    greet(z > 0, zdev(jnp.maximum(z - 1, 0)))
    greet(z + HOPS <= top, zdev(jnp.minimum(z + HOPS, top)))
    greet(z == 0, zdev(top))
    one = jnp.int32(1)
    none = jnp.int32(0)
    callers = 4 + jnp.where(z < top, one, none) + jnp.where(z > 0, one, none)
    callers = callers + jnp.where(z >= HOPS, one, none)
    callers = callers + jnp.where(z == top, one, none)
    pl.semaphore_wait(barrier, callers)

    @pl.when(z >= HOPS)
    def _():
        tell(chain_ready, zdev(jnp.maximum(z - HOPS, 0)))

    @pl.when(z == top)
    def _():
        tell(wrap_ready, zdev(0))

    s_wz, s_wx, s_wr, s_wp, s_act, s_own, s_chain, s_pe = (send_sem.at[k] for k in range(8))
    s_tm = [send_sem.at[9 + r] for r in range(HOPS)]
    s_kvo = [send_sem.at[9 + HOPS + k] for k in range(2)]

    def send_kv(d, i, kind):
        piece = kv.at[kind, chip_from(d, i) * 2 + c]
        send(piece, piece, skz_sem.at[d, i, kind], kvz_sem.at[d, i + 1, kind], ring[d])

    def send_w(d, i):
        piece = wbuf.at[0, chip_from(d, i) * 2 + c]
        send(piece, piece, s_wz, wz_sem.at[d, i + 1], ring[d])

    loads[0].wait()
    loads[1].wait()
    for kind in range(2):
        for d in range(2):

            @pl.when(kv_out(d, 0) & ((z > 0) | (d == 0)))
            def _():
                send_kv(d, jnp.int32(0), kind)

        mine = kv.at[kind, sp]
        send(mine, mine, s_kvo[kind], kvo_sem.at[kind], partner)
    loads[2].wait()
    mine = wbuf.at[0, sp]
    send_w(0, jnp.int32(0))

    @pl.when(z > 0)
    def _():
        send_w(1, jnp.int32(0))

    send(mine, mine, s_wp, wp_sem.at[0], partner)
    send(mine, wbuf.at[3, sp], s_wx, wx_sem.at[1, 0, 0], xdev(1))
    send(mine, wbuf.at[1, sp], s_wx, wx_sem.at[0, 0, 0], xdev(-1))

    floor_rate = jax.nn.sigmoid(-lb[...])
    inflow = floor_rate * jax.nn.sigmoid(-fg[...].astype(f32))
    one_less = 1.0 - inflow
    add2 = added[...]
    add_wide = jnp.concatenate(
        [jnp.broadcast_to(add2[:, h : h + 1], (tok, HEAD)) for h in range(2)], axis=1
    )
    log_decay = jnp.log(one_less) - ((one_less - 1.0) + inflow) / one_less + add_wide
    row = lax.broadcasted_iota(jnp.int32, (tok, tok), 0)
    col = lax.broadcasted_iota(jnp.int32, (tok, tok), 1)
    tri = jnp.where(col <= row, 1.0, 0.0).astype(f32)
    cum = dot(tri, log_decay, precision=lax.Precision.HIGHEST)
    last = cum[tok - 1 : tok, :]
    kin = (inflow * jnp.exp(last - cum)).astype(bf16)
    through = jnp.exp(last)
    r16 = lax.broadcasted_iota(jnp.int32, (16, HEAD), 0)

    def pack_decay(dec):
        hi = dec.astype(bf16)
        lo = (dec - hi.astype(f32)).astype(bf16)
        zero = jnp.zeros((16, HEAD), f32)
        return jnp.where(
            r16 == 0, hi.astype(f32), jnp.where(r16 == 1, lo.astype(f32), zero)
        ).astype(bf16)

    def unpack_decay(msg):
        rows = msg[HEAD : HEAD + 16, :].astype(f32)
        return rows[0:1] + rows[1:2]

    def unpack_state(msg):
        return msg[0:HEAD, :].astype(f32)

    for h in range(2):
        cols = slice(h * HEAD, (h + 1) * HEAD)
        st = dot(rv[:, cols], kin[:, cols], TN)
        dev_state[h] = st
        dev_decay[h] = through[:, cols]
        sown[h, 0:HEAD, :] = st.astype(bf16)
        sown[h, HEAD : HEAD + 16, :] = pack_decay(through[:, cols])
    send(sown, spart, s_own, st_sem.at[0], partner)

    got(spart, st_sem.at[0])
    own_s, own_d = dev_state[c], dev_decay[c]
    oth_s, oth_d = unpack_state(spart[c]), unpack_decay(spart[c])
    late_d = jnp.where(up, oth_d, own_d)
    chip_state = late_d * jnp.where(up, own_s, oth_s) + jnp.where(up, oth_s, own_s)
    tm[0, 0:HEAD, :] = chip_state.astype(bf16)
    tm[0, HEAD : HEAD + 16, :] = pack_decay(own_d * oth_d)
    above = zdev(jnp.minimum(z + 1, top))

    @pl.when(z < top)
    def _():
        send(tm.at[0], tm.at[1], s_tm[0], st_sem.at[1], above)

    qe[...] = (rq[...].astype(f32) * jnp.exp(cum)).astype(bf16)

    def local_outputs():
        r64 = lax.broadcasted_iota(jnp.int32, (BLK, BLK), 0)
        c64 = lax.broadcasted_iota(jnp.int32, (BLK, BLK), 1)
        for h in range(2):
            cols = slice(h * HEAD, (h + 1) * HEAD)
            state = None
            for b in range(tok // BLK):
                rows = slice(b * BLK, (b + 1) * BLK)
                blk_cum = cum[rows, cols]
                if b:
                    blk_cum = blk_cum - cum[b * BLK - 1 : b * BLK, cols]
                qd = (rq[rows, cols].astype(f32) * jnp.exp(blk_cum)).astype(bf16)
                kd = (inflow[rows, cols] * jnp.exp(-blk_cum)).astype(bf16)
                scores = dot(qd, kd, NT)
                scores = jnp.where(c64 <= r64, scores, 0.0).astype(bf16)
                res = dot(scores, rv[rows, cols])
                if b:
                    res = res + dot(qd, state.astype(bf16), NT)
                loc[rows, cols] = res
                if b + 1 < tok // BLK:
                    end = blk_cum[BLK - 1 : BLK, :]
                    ke = (inflow[rows, cols] * jnp.exp(end - blk_cum)).astype(bf16)
                    new = dot(rv[rows, cols], ke, TN)
                    state = new if b == 0 else state * jnp.exp(end) + new

    ones = jnp.ones((16, 2 * tok), bf16)

    def pair_update(chip, fresh):
        s0 = chip * 2
        keys = kv[0, pl.ds(s0, 2)].reshape(2 * tok, HEAD)
        vt = jnp.concatenate(
            [
                kv[1, s0, 0:HEAD, :], kv[1, s0, HEAD : 2 * HEAD, :],
                kv[1, s0 + 1, 0:HEAD, :], kv[1, s0 + 1, HEAD : 2 * HEAD, :],
            ],
            axis=1,
        )
        vt = jnp.concatenate([vt, ones], axis=0)
        scores = [dot(keys, qp[t], NT) for t in range(4)]
        for t in range(4):
            s = scores[t]
            if fresh:
                kpos = lax.broadcasted_iota(jnp.int32, s.shape, 0)
                qpos = lax.broadcasted_iota(jnp.int32, s.shape, 1) + c * tok
                s = jnp.where(kpos <= qpos, s, -1e30)
                new_max = jnp.max(s, axis=0, keepdims=True)
                w = jnp.where(kpos <= qpos, jnp.exp(s - new_max), 0.0).astype(bf16)
                acc[t] = dot(vt, w)
            else:
                old_max = mrow[t]
                new_max = jnp.maximum(old_max, jnp.max(s, axis=0, keepdims=True))
                w = jnp.exp(s - new_max).astype(bf16)
                acc[t] = acc[t] * jnp.exp(old_max - new_max) + dot(vt, w)
            mrow[t] = new_max

    def forward_w(d, u):
        i = item(d, u)

        @pl.when((i >= 1) & (i <= w_far[d]))
        def _():
            s = chip_from(d, i) * 2 + c
            piece = wbuf.at[0, s]
            got(piece, wz_sem.at[d, i])

            @pl.when((i < w_far[d]) & ((z > 0) | (u >= meet) | (d == 0)))
            def _():
                send_w(d, i)

            send(piece, wbuf.at[3, s], s_wx, wx_sem.at[1, d, i], xdev(1))
            send(piece, wbuf.at[1, s], s_wx, wx_sem.at[0, d, i], xdev(-1))
            send(piece, piece, s_wp, wp_sem.at[0], partner)

    def spread_w(d, u):
        j = item(d, u - 2)

        @pl.when((j >= d) & (j <= w_far[d]) & (u >= 2))
        def _():
            s = chip_from(d, j) * 2 + c
            for k in range(2):
                ref = wbuf.at[2 * k + 1, s]
                got(ref, wx_sem.at[k, d, j])
                send(ref, ref, s_wp, wp_sem.at[0], partner)
            send(wbuf.at[3 - 2 * c, s], wbuf.at[2, s], s_wr, wr_sem.at[d, j], xdev(1 - 2 * c))

        q = item(d, u - 4)

        @pl.when((q >= d) & (q <= w_far[d]) & (u >= 4))
        def _():
            ref = wbuf.at[2, chip_from(d, q) * 2 + c]
            got(ref, wr_sem.at[d, q])
            send(ref, ref, s_wp, wp_sem.at[0], partner)

    def forward_kv(d, u, kind):
        i = item(d, u)

        @pl.when(kv_in(d, i))
        def _():
            piece = kv.at[kind, chip_from(d, i) * 2 + c]
            got(piece, kvz_sem.at[d, i, kind])

            @pl.when(kv_out(d, i) & ((z > 0) | (u >= meet) | (d == 0)))
            def _():
                send_kv(d, i, kind)

            @pl.when(kv_used(d, i))
            def _():
                send(piece, piece, skp_sem.at[d, i, kind], kvp_sem.at[d, i, kind], partner)

    def take(d, u):
        i = item(d, u - 1)

        @pl.when(kv_used(d, i) & (u >= 1))
        def _():
            chip = chip_from(d, i)
            for kind in range(2):
                got(kv.at[kind, chip * 2 + 1 - c], kvp_sem.at[d, i, kind])
            pair_update(chip, False)

    def meet_top(u):
        @pl.when((z == 0) & (u == meet))
        def _():
            pl.semaphore_wait(wrap_ready, 1)

            def late(k, carry):
                send_w(1, k)
                for kind in range(2):

                    @pl.when(kv_out(1, k))
                    def _():
                        send_kv(1, k, kind)

                return carry

            lax.fori_loop(0, meet, late, 0)

    def hand_out(src, which):
        for r in range(1, 4):
            d = (x - r + ntp) % ntp
            rows = src.at[pl.ds(pl.multiple_of(d * rows_out, rows_out), rows_out)]
            send(rows, ract.at[which, r], s_act, act_sem.at[which, r], (g, sp, d))

    late_turn = jnp.maximum((z - 3 * HOPS) // HOPS, 0)
    turn = HOPS + 1 + late_turn

    def state_steps(i):
        @pl.when((i >= 1) & (i <= HOPS) & (z >= i))
        def _():
            got(tm.at[i], st_sem.at[i])

            @pl.when((i < HOPS) & (z < top))
            def _():
                send(tm.at[i], tm.at[i + 1], send_sem.at[9 + i], st_sem.at[i + 1], above)

        @pl.when(i == turn)
        def _():
            @pl.when(z >= HOPS)
            def _():
                got(ch.at[0], st_sem.at[HOPS + 1])

            state = unpack_state(ch[0])
            for r in range(HOPS, 0, -1):
                state = state * unpack_decay(tm[r]) + unpack_state(tm[r])
            ch[1, 0:HEAD, :] = state.astype(bf16)
            send(ch.at[1], pe, s_pe, st_sem.at[HOPS + 2], partner)

            @pl.when(z + HOPS <= top)
            def _():
                pl.semaphore_wait(chain_ready, 1)
                send(
                    ch.at[1], ch.at[0], s_chain, st_sem.at[HOPS + 1],
                    zdev(jnp.minimum(z + HOPS, top)),
                )

        @pl.when(i == turn + 1)
        def _():
            got(pe, st_sem.at[HOPS + 2])
            ours, theirs = unpack_state(ch[1]), unpack_state(pe[...])
            for h in range(2):
                cols = slice(h * HEAD, (h + 1) * HEAD)
                before = jnp.where(c == h, ours, theirs)
                second = before * unpack_decay(spart[h]) + unpack_state(spart[h])
                before = jnp.where(up, before, second).astype(bf16)
                mix = loc[:, cols] + dot(qe[:, cols], before, NT)
                mean_square = jnp.mean(mix * mix, axis=-1, keepdims=True)
                arec[:, cols] = (mix * lax.rsqrt(mean_square + EPS) * rgain[...]).astype(bf16)
            hand_out(arec, 0)

    def step(u, carry):
        meet_top(u)
        for d in range(2):
            forward_w(d, u)
        for d in range(2):
            forward_kv(d, u, 0)
        state_steps(u)
        take(0, u)
        for d in range(2):
            forward_kv(d, u, 1)
        for d in range(2):
            spread_w(d, u)
        take(1, u)

        @pl.when(u == 0)
        def _():
            local_outputs()
            for kind in range(2):
                got(kv.at[kind, z * 2 + 1 - c], kvo_sem.at[kind])
            pair_update(z, True)

        return carry

    lax.fori_loop(0, half + half // 2 + 7, step, 0)

    for h in range(2):
        cols = slice(h * HEAD, (h + 1) * HEAD)
        first, second = acc[h], acc[2 + h]
        mix = first[0:HEAD] / first[HEAD : HEAD + 1]
        mix = mix - lam[h : h + 1, 0:1] * (second[0:HEAD] / second[HEAD : HEAD + 1])
        mean_square = jnp.mean(mix * mix, axis=0, keepdims=True)
        mix = jnp.transpose(mix * lax.rsqrt(mean_square + EPS))
        aatt[:, cols] = (mix * again[...]).astype(bf16)
    hand_out(aatt, 1)

    got(wbuf.at[0:4, 0:nz], wp_sem.at[0])
    chunk = 512
    pieces = chunk // 32

    def project(which, src):
        own_rows = src[pl.ds(pl.multiple_of(x * rows_out, rows_out), rows_out), :]
        acts = [own_rows if r == 0 else ract[which, r] for r in range(4)]

        def columns(n):
            total = None
            for r in range(4):
                w = [
                    wbuf[
                        r, pl.ds(n * pieces, pieces),
                        which * 64 + kb * 32 : which * 64 + kb * 32 + 32, :
                    ].reshape(chunk, HEAD)
                    for kb in range(2)
                ]
                term = dot(acts[r], jnp.concatenate(w, axis=1), NT)
                total = term if total is None else total + term
            return total

        return columns

    for r in range(1, 4):
        got(ract.at[0, r], act_sem.at[0, r])
    rec = project(0, arec)
    for n in range(2048 // chunk):
        part[:, n * chunk : (n + 1) * chunk] = rec(n)
    for r in range(1, 4):
        got(ract.at[1, r], act_sem.at[1, r])
    att = project(1, aatt)
    for n in range(2048 // chunk):
        cols = slice(n * chunk, (n + 1) * chunk)
        out[:, cols] = (part[:, cols] + att(n)).astype(bf16)

    def drain(i, carry):
        for d in range(2):
            for kind in range(2):

                @pl.when(kv_out(d, i))
                def _():
                    got(kv.at[kind, 0], skz_sem.at[d, i, kind])

                @pl.when(kv_used(d, i))
                def _():
                    got(kv.at[kind, 0], skp_sem.at[d, i, kind])

        return carry

    lax.fori_loop(0, kv_up + 1, drain, 0)
    for kind in range(2):
        got(kv.at[kind, 0], s_kvo[kind])
    got(wbuf.at[0, 0 : nz - 1], s_wz)
    got(wbuf.at[0:2, 0:nz], s_wx)
    got(wbuf.at[0, 0:nz], s_wr)
    got(wbuf.at[0:4, 0:nz], s_wp)
    got(sown, s_own)
    got(pe, s_pe)

    @pl.when(z + HOPS <= top)
    def _():
        got(pe, s_chain)

    for r in range(HOPS):

        @pl.when((z < top) & (z >= r))
        def _():
            got(pe, s_tm[r])

    got(ract.at[0:2, 1:4], s_act)


def shards(rq, fg, rv, lb, added, rgain, q1, k1, q2, k2, v, lam, again, w, *, nz):
    tok = rq.shape[0]
    half_tok = tok // 2
    keys = jnp.concatenate([k1, k2], axis=1)
    vt = v.reshape(2, half_tok, HEAD).transpose(0, 2, 1).reshape(tok, HEAD)
    kvl = jnp.stack([keys, vt])
    wl = w.reshape(2, 2, HEAD, 32).transpose(0, 1, 3, 2).reshape(HEAD, HEAD)
    scale = jnp.asarray(DA_HD**-0.5, bf16)
    zero = jnp.zeros((tok, DA_HD), bf16)
    qp = jnp.stack(
        [
            jnp.concatenate([q1[:, :DA_HD] * scale, zero], axis=1),
            jnp.concatenate([q1[:, DA_HD:] * scale, zero], axis=1),
            jnp.concatenate([zero, q2[:, :DA_HD] * scale], axis=1),
            jnp.concatenate([zero, q2[:, DA_HD:] * scale], axis=1),
        ]
    )
    vmem = pl.BlockSpec(memory_space=pltpu.VMEM)
    hbm = pl.BlockSpec(memory_space=pltpu.HBM)
    nsp = 2 * nz
    msg = (HEAD + 16, HEAD)
    dma = pltpu.SemaphoreType.DMA
    return pl.pallas_call(
        functools.partial(kernel, nz),
        out_shape=jax.ShapeDtypeStruct((tok // 4, w.shape[2] * nsp), bf16),
        in_specs=[hbm, hbm] + [vmem] * 9,
        out_specs=vmem,
        scratch_shapes=[
            pltpu.VMEM((2, nsp, tok, HEAD), bf16),
            pltpu.VMEM((4, nsp, HEAD, HEAD), bf16),
            pltpu.VMEM((4, HEAD + 16, tok), f32),
            pltpu.VMEM((4, 1, tok), f32),
            pltpu.VMEM((2,) + msg, bf16),
            pltpu.VMEM((2,) + msg, bf16),
            pltpu.VMEM((HOPS + 1,) + msg, bf16),
            pltpu.VMEM((2,) + msg, bf16),
            pltpu.VMEM(msg, bf16),
            pltpu.VMEM((tok, 2 * HEAD), f32),
            pltpu.VMEM((tok, 2 * HEAD), bf16),
            pltpu.VMEM((2, HEAD, HEAD), f32),
            pltpu.VMEM((2, 1, HEAD), f32),
            pltpu.VMEM((tok, 2 * HEAD), bf16),
            pltpu.VMEM((tok, 2 * HEAD), bf16),
            pltpu.VMEM((2, 4, tok // 4, 2 * HEAD), bf16),
            pltpu.VMEM((tok // 4, w.shape[2] * nsp), f32),
            dma((3,)),
            dma((11 + HOPS,)),
            dma((2, (5 * nz) // 8 + 2, 2)),
            dma((2, (5 * nz) // 8 + 2, 2)),
            dma((2, (5 * nz) // 8 + 2, 2)),
            dma((2, (5 * nz) // 8 + 2, 2)),
            dma((2,)),
            dma((2, nz // 2 + 2)),
            dma((2, 2, nz // 2 + 1)),
            dma((2, nz // 2 + 1)),
            dma((1,)),
            dma((HOPS + 3,)),
            dma((2, 4)),
            pltpu.SemaphoreType.REGULAR,
            pltpu.SemaphoreType.REGULAR,
        ],
        compiler_params=pltpu.CompilerParams(
            collective_id=0, has_side_effects=True, vmem_limit_bytes=60 * 1024 * 1024
        ),
    )(
        kvl, wl, qp, rq, fg, rv, lb.reshape(1, -1), added,
        jnp.broadcast_to(lam[:, None], (2, HEAD)), rgain.reshape(1, -1), again.reshape(1, -1),
    )


def solution(mesh):
    tokens = P(("grp", "sp"), "tp")
    return jax.shard_map(
        functools.partial(shards, nz=mesh.shape["sp"] // 2),
        mesh=mesh,
        in_specs=(
            tokens, tokens, tokens, P("tp"), tokens, P(),
            tokens, tokens, tokens, tokens, tokens, P("tp"), P(), P(None, "tp", "sp"),
        ),
        out_specs=P(("grp", "sp", "tp"), None),
        check_vma=False,
    )
```

time: 155 us -> 173 us (1.12)
  Pallas kernels: 146 us -> 164 us
    pallas_call x1, Pallas kernels: 146 us -> 164 us  [shards(): pl.pallas_call(functools.partial(kernel, nz), out_shape=jax.ShapeDtypeStr...]
where the time goes in v2:
time: 173 us
  Pallas kernels  164 us (95%)
  local copies, waits for them, and re-layouts  7.25 us (4%)
    pallas_call x1, Pallas kernels, shards(): pl.pallas_call(functools.partial(kernel, nz), out_shape=jax.ShapeDtypeStr...  164 us
    unnamed x20, local copies, waits for them, and re-layouts  5.75 us

profile of v2, /device:TPU:33, one launch (start us, length us, event | category | flops | bytes accessed | tf_op | source)
XLA Modules:
  0.0 172.8 jit_solution(4833833482941348865)
XLA Ops:
  0.0 0.0 copy-start
  0.0 0.0 copy-start.7
  0.0 0.7 copy-done.7
  0.7 0.6 broadcast_in_dim.2.lam
  1.3 0.0 copy-done
  1.3 0.0 copy-start.4
  1.3 0.6 copy_bitcast_fusion
  1.9 0.2 copy-done.4
  2.1 0.0 copy-start.5
  2.1 0.1 copy.15
  2.2 0.6 copy-done.5
  2.8 0.1 copy.16
  2.9 0.0 copy-start.3
  3.0 0.1 maximum_bitcast_fusion
  3.1 0.7 copy-done.3
  3.8 0.1 copy.17
  3.9 0.0 copy-start.6
  3.9 0.7 pad_maximum_fusion.1.kvl
  4.6 0.0 copy-done.6
  4.6 0.0 copy-start.1
  4.6 0.8 copy.19.added
  5.4 0.1 copy-done.1
  5.4 0.1 slice_multiply_fusion.3
  5.5 0.0 copy-start.2
  5.6 0.8 copy-done.2
  6.4 0.1 slice_multiply_fusion.1
  6.5 0.1 pad_bitcast_fusion
  6.6 0.7 pad_maximum_fusion.qp
  7.3 163.8 %shard_map.136 = bf16[64,2048]{1,0:T(8,128)(2,1)} custom-call(bf16[2,256,128]{2,1,0:T(8,128)(2,1)} %pad_maximum_fusion.1.kvl, bf16[128,128]{1,0:T(8,128)(2,1)} %bitcast.26, bf16[4,256,128]{2,1,0:T(8,128)(2,1)} %pad_maximum_fusion.qp, bf16[256,256]{1,0:T(8,128)(2,1)} %rq.1, bf16[256,256]{1,0:T(8,128)(2,1)} %fg.1, bf16[256,256]{1,0:T(8,128)(2,1)} %rv.1, ...), custom_call_target="tpu_custom_call" | custom-call | tf_op jit(solution)/shard_map/pallas_call | solution.py:537
  171.1 1.7 copy.23
  (1 shorter events, 0.0 us)
Async XLA Ops:
  0.0 1.3 copy-start
  0.0 0.7 copy-start.7
  1.3 0.8 copy-start.4
  2.1 0.8 copy-start.5
  2.9 0.8 copy-start.3
  3.9 0.7 copy-start.6
  4.6 0.8 copy-start.1
  5.5 0.8 copy-start.2

commit v3 on v2

--- a/solution.py
+++ b/solution.py
@@ -22,7 +22,8 @@
 
 
 def kernel(
-    nz, kvl, wl, qp, rq, fg, rv, lb, added, lam, rgain, again, out,
+    nz, kvl, wl, qp_in, rq_in, fg_in, rv_in, lb, added, lam, rgain, again, out,
+    qp, rq, fg, rv,
     kv, wbuf, acc, mrow, sown, spart, tm, ch, pe, loc, qe, dev_state, dev_decay,
     arec, aatt, ract, part,
     copy_sem, send_sem, skz_sem, skp_sem, kvz_sem, kvp_sem, kvo_sem, wz_sem, wx_sem, wr_sem,
@@ -34,11 +35,11 @@
     up = c == 0
     top = nz - 1
     half = nz // 2
-    kv_up = (5 * nz) // 8
+    kv_up = (21 * nz) // 32
     kv_wrap = nz - 1 - kv_up
     w_far = (half, half - 1)
-    gap = jnp.maximum(half // 2 + 1 - z, 0)
-    meet = 10
+    gap = jnp.maximum(1 - z, 0)
+    meet = 1
     tok = rq.shape[0]
     rows_out = tok // ntp
     mesh_id = pl.DeviceIdType.MESH
@@ -72,6 +73,19 @@
             return u
         return jnp.where(u <= z, u, jnp.where(u > z + gap, u - gap, -1))
 
+    def w_item(d, u, v):
+        if d == 1:
+            return u if v == 0 else jnp.int32(-1)
+        low = item(0, u) if v == 0 else jnp.int32(-1)
+        low = jnp.where(u > z + gap, z + 2 * (u - z - gap) - 1 + v, low)
+        near = z - half
+        steps = (near + 1) // 2
+        fast = jnp.where((u >= 1) & (2 * u - 1 + v <= near), 2 * u - 1 + v, u if v == 0 else -1)
+        fast = jnp.where((u >= 1) & (v == 1) & (2 * u > near), -1, fast)
+        slow = near + u - steps if v == 0 else jnp.int32(-1)
+        high = jnp.where(u <= steps, fast, slow)
+        return jnp.where(z < half, low, high)
+
     def kv_used(d, i):
         if d == 0:
             return (i >= 1) & (i <= kv_up) & (z >= i)
@@ -92,6 +106,8 @@
 
     loads = [pltpu.make_async_copy(kvl.at[k], kv.at[k, sp], copy_sem.at[k]) for k in range(2)]
     loads.append(pltpu.make_async_copy(wl, wbuf.at[0, sp], copy_sem.at[2]))
+    for k, (src, dst) in enumerate(((fg_in, fg), (rv_in, rv), (rq_in, rq), (qp_in, qp))):
+        loads.append(pltpu.make_async_copy(src, dst, copy_sem.at[3 + k]))
     for load in loads:
         load.start()
     tm[...] = jnp.zeros_like(tm)
@@ -161,6 +177,8 @@
     send(mine, wbuf.at[3, sp], s_wx, wx_sem.at[1, 0, 0], xdev(1))
     send(mine, wbuf.at[1, sp], s_wx, wx_sem.at[0, 0, 0], xdev(-1))
 
+    for load in loads[3:]:
+        load.wait()
     floor_rate = jax.nn.sigmoid(-lb[...])
     inflow = floor_rate * jax.nn.sigmoid(-fg[...].astype(f32))
     one_less = 1.0 - inflow
@@ -272,8 +290,8 @@
                 acc[t] = acc[t] * jnp.exp(old_max - new_max) + dot(vt, w)
             mrow[t] = new_max
 
-    def forward_w(d, u):
-        i = item(d, u)
+    def forward_w(d, u, v):
+        i = w_item(d, u, v)
 
         @pl.when((i >= 1) & (i <= w_far[d]))
         def _():
@@ -289,8 +307,8 @@
             send(piece, wbuf.at[1, s], s_wx, wx_sem.at[0, d, i], xdev(-1))
             send(piece, piece, s_wp, wp_sem.at[0], partner)
 
-    def spread_w(d, u):
-        j = item(d, u - 2)
+    def spread_w(d, u, v):
+        j = w_item(d, u - 2, v)
 
         @pl.when((j >= d) & (j <= w_far[d]) & (u >= 2))
         def _():
@@ -301,7 +319,7 @@
                 send(ref, ref, s_wp, wp_sem.at[0], partner)
             send(wbuf.at[3 - 2 * c, s], wbuf.at[2, s], s_wr, wr_sem.at[d, j], xdev(1 - 2 * c))
 
-        q = item(d, u - 4)
+        q = w_item(d, u - 4, v)
 
         @pl.when((q >= d) & (q <= w_far[d]) & (u >= 4))
         def _():
@@ -358,8 +376,8 @@
             rows = src.at[pl.ds(pl.multiple_of(d * rows_out, rows_out), rows_out)]
             send(rows, ract.at[which, r], s_act, act_sem.at[which, r], (g, sp, d))
 
-    late_turn = jnp.maximum((z - 3 * HOPS) // HOPS, 0)
-    turn = HOPS + 1 + late_turn
+    late_turn = half + jnp.maximum((z - half - HOPS) // HOPS, 0)
+    turn = jnp.where(z < half, z + 1, late_turn)
 
     def state_steps(i):
         @pl.when((i >= 1) & (i <= HOPS) & (z >= i))
@@ -406,16 +424,16 @@
 
     def step(u, carry):
         meet_top(u)
-        for d in range(2):
-            forward_w(d, u)
+        for d, v in ((0, 0), (1, 0), (0, 1)):
+            forward_w(d, u, v)
         for d in range(2):
             forward_kv(d, u, 0)
         state_steps(u)
         take(0, u)
         for d in range(2):
             forward_kv(d, u, 1)
-        for d in range(2):
-            spread_w(d, u)
+        for d, v in ((0, 0), (1, 0), (0, 1)):
+            spread_w(d, u, v)
         take(1, u)
 
         @pl.when(u == 0)
@@ -427,7 +445,7 @@
 
         return carry
 
-    lax.fori_loop(0, half + half // 2 + 7, step, 0)
+    lax.fori_loop(0, half + 8, step, 0)
 
     for h in range(2):
         cols = slice(h * HEAD, (h + 1) * HEAD)
@@ -537,9 +555,13 @@
     return pl.pallas_call(
         functools.partial(kernel, nz),
         out_shape=jax.ShapeDtypeStruct((tok // 4, w.shape[2] * nsp), bf16),
-        in_specs=[hbm, hbm] + [vmem] * 9,
+        in_specs=[hbm] * 6 + [vmem] * 5,
         out_specs=vmem,
         scratch_shapes=[
+            pltpu.VMEM((4, tok, HEAD), bf16),
+            pltpu.VMEM((tok, 2 * HEAD), bf16),
+            pltpu.VMEM((tok, 2 * HEAD), bf16),
+            pltpu.VMEM((tok, 2 * HEAD), bf16),
             pltpu.VMEM((2, nsp, tok, HEAD), bf16),
             pltpu.VMEM((4, nsp, HEAD, HEAD), bf16),
             pltpu.VMEM((4, HEAD + 16, tok), f32),
@@ -557,12 +579,12 @@
             pltpu.VMEM((tok, 2 * HEAD), bf16),
             pltpu.VMEM((2, 4, tok // 4, 2 * HEAD), bf16),
             pltpu.VMEM((tok // 4, w.shape[2] * nsp), f32),
-            dma((3,)),
+            dma((7,)),
             dma((11 + HOPS,)),
-            dma((2, (5 * nz) // 8 + 2, 2)),
-            dma((2, (5 * nz) // 8 + 2, 2)),
-            dma((2, (5 * nz) // 8 + 2, 2)),
-            dma((2, (5 * nz) // 8 + 2, 2)),
+            dma((2, (21 * nz) // 32 + 2, 2)),
+            dma((2, (21 * nz) // 32 + 2, 2)),
+            dma((2, (21 * nz) // 32 + 2, 2)),
+            dma((2, (21 * nz) // 32 + 2, 2)),
             dma((2,)),
             dma((2, nz // 2 + 2)),
             dma((2, 2, nz // 2 + 1)),

time: 173 us -> 135 us (0.78)
  Pallas kernels: 164 us -> 126 us
    pallas_call x1, Pallas kernels: 164 us -> 126 us  [shards(): pl.pallas_call(functools.partial(kernel, nz), out_shape=jax.ShapeDtypeStr...]
where the time goes in v3:
time: 135 us
  Pallas kernels  126 us (93%)
  local copies, waits for them, and re-layouts  7.25 us (5%)
  other arithmetic  1.68 us (1%)
    pallas_call x1, Pallas kernels, shards(): pl.pallas_call(functools.partial(kernel, nz), out_shape=jax.ShapeDtypeStr...  126 us
    unnamed x20, local copies, waits for them, and re-layouts  5.75 us

profile of v3, /device:TPU:33, one launch (start us, length us, event | category | flops | bytes accessed | tf_op | source)
XLA Modules:
  0.0 134.5 jit_solution(8026436302649473429)
XLA Ops:
  0.0 0.0 copy-start
  0.0 0.0 copy-start.7
  0.0 0.7 copy-done.7
  0.7 0.6 broadcast_in_dim.2.lam
  1.3 0.0 copy-done
  1.3 0.0 copy-start.4
  1.3 0.6 copy_bitcast_fusion
  1.9 0.2 copy-done.4
  2.1 0.0 copy-start.5
  2.1 0.1 copy.15
  2.2 0.6 copy-done.5
  2.8 0.1 copy.16
  2.9 0.0 copy-start.3
  3.0 0.1 maximum_bitcast_fusion
  3.1 0.7 copy-done.3
  3.8 0.1 copy.17
  3.9 0.0 copy-start.6
  3.9 0.7 pad_maximum_fusion.1.kvl
  4.6 0.0 copy-done.6
  4.6 0.0 copy-start.1
  4.6 0.8 copy.19.added
  5.4 0.1 copy-done.1
  5.4 0.1 slice_multiply_fusion.3
  5.5 0.0 copy-start.2
  5.6 0.8 copy-done.2
  6.4 0.1 slice_multiply_fusion.1
  6.5 0.1 pad_bitcast_fusion
  6.6 0.7 pad_maximum_fusion.qp_in
  7.3 125.5 %shard_map.136 = bf16[64,2048]{1,0:T(8,128)(2,1)} custom-call(bf16[2,256,128]{2,1,0:T(8,128)(2,1)} %pad_maximum_fusion.1.kvl, bf16[128,128]{1,0:T(8,128)(2,1)} %bitcast.26, bf16[4,256,128]{2,1,0:T(8,128)(2,1)} %pad_maximum_fusion.qp_in, bf16[256,256]{1,0:T(8,128)(2,1)} %rq_in.1, bf16[256,256]{1,0:T(8,128)(2,1)} %fg_in.1, bf16[256,256]{1,0:T(8,128)(2,1)} %rv_in.1, ...), custom_call_target="tpu_custom_call" | custom-call | tf_op jit(solution)/shard_map/pallas_call | solution.py:555
  132.8 1.7 %copy.23 = bf16[64,2048]{1,0:T(8,128)(2,1)} copy(bf16[64,2048]{1,0:T(8,128)(2,1)} %shard_map.136) | data formatting | bytes 524288
  (1 shorter events, 0.0 us)
Async XLA Ops:
  0.0 1.3 copy-start
  0.0 0.7 copy-start.7
  1.3 0.8 copy-start.4
  2.1 0.8 copy-start.5
  2.9 0.8 copy-start.3
  3.9 0.7 copy-start.6
  4.6 0.8 copy-start.1
  5.5 0.8 copy-start.2

commit v4 on v3

--- a/solution.py
+++ b/solution.py
@@ -422,6 +422,19 @@
                 arec[:, cols] = (mix * lax.rsqrt(mean_square + EPS) * rgain[...]).astype(bf16)
             hand_out(arec, 0)
 
+    def finish_attention():
+        for h in range(2):
+            cols = slice(h * HEAD, (h + 1) * HEAD)
+            first, second = acc[h], acc[2 + h]
+            mix = first[0:HEAD] / first[HEAD : HEAD + 1]
+            mix = mix - lam[0:1, h : h + 1] * (second[0:HEAD] / second[HEAD : HEAD + 1])
+            mean_square = jnp.mean(mix * mix, axis=0, keepdims=True)
+            mix = jnp.transpose(mix * lax.rsqrt(mean_square + EPS))
+            aatt[:, cols] = (mix * again[...]).astype(bf16)
+        hand_out(aatt, 1)
+
+    final = jnp.minimum(z, kv_up) + 2
+
     def step(u, carry):
         meet_top(u)
         for d, v in ((0, 0), (1, 0), (0, 1)):
@@ -443,19 +456,13 @@
                 got(kv.at[kind, z * 2 + 1 - c], kvo_sem.at[kind])
             pair_update(z, True)
 
+        @pl.when(u == final)
+        def _():
+            finish_attention()
+
         return carry
 
     lax.fori_loop(0, half + 8, step, 0)
-
-    for h in range(2):
-        cols = slice(h * HEAD, (h + 1) * HEAD)
-        first, second = acc[h], acc[2 + h]
-        mix = first[0:HEAD] / first[HEAD : HEAD + 1]
-        mix = mix - lam[h : h + 1, 0:1] * (second[0:HEAD] / second[HEAD : HEAD + 1])
-        mean_square = jnp.mean(mix * mix, axis=0, keepdims=True)
-        mix = jnp.transpose(mix * lax.rsqrt(mean_square + EPS))
-        aatt[:, cols] = (mix * again[...]).astype(bf16)
-    hand_out(aatt, 1)
 
     got(wbuf.at[0:4, 0:nz], wp_sem.at[0])
     chunk = 512
@@ -600,7 +607,7 @@
         ),
     )(
         kvl, wl, qp, rq, fg, rv, lb.reshape(1, -1), added,
-        jnp.broadcast_to(lam[:, None], (2, HEAD)), rgain.reshape(1, -1), again.reshape(1, -1),
+        lam.reshape(1, -1), rgain.reshape(1, -1), again.reshape(1, -1),
     )
 
 

time: 135 us -> 135 us (level)
    unnamed x20 -> x18, local copies, waits for them, and re-layouts: 5.75 us -> 5.83 us
where the time goes in v4:
time: 135 us; the launch traced here: 134 us
  Pallas kernels  126 us (93%)
  local copies, waits for them, and re-layouts  6.69 us (5%)
  other arithmetic  1.68 us (1%)
    pallas_call x1, Pallas kernels, shards(): pl.pallas_call(functools.partial(kernel, nz), out_shape=jax.ShapeDtypeStr...  126 us
    unnamed x18, local copies, waits for them, and re-layouts  5.83 us

profile of v4, /device:TPU:33, one launch (start us, length us, event | category | flops | bytes accessed | tf_op | source)
XLA Modules:
  0.0 134.0 jit_solution(3123560914202341256)
XLA Ops:
  0.0 0.0 copy-start
  0.0 0.8 copy-done
  0.8 0.0 copy-start.4
  0.8 0.6 copy_bitcast_fusion
  1.4 0.1 copy-done.4
  1.5 0.0 copy-start.5
  1.5 0.1 copy.15
  1.6 0.6 copy-done.5
  2.3 0.1 copy.16
  2.4 0.0 copy-start.3
  2.4 0.1 maximum_bitcast_fusion
  2.5 0.7 copy-done.3
  3.2 0.1 copy.17
  3.4 0.0 copy-start.6
  3.4 0.7 pad_maximum_fusion.1.kvl
  4.0 0.0 copy-done.6
  4.1 0.0 copy-start.1
  4.1 0.8 copy.19.added
  4.8 0.0 copy-done.1
  4.9 0.1 slice_multiply_fusion.3
  5.0 0.0 copy-start.2
  5.0 0.8 copy-done.2
  5.8 0.1 slice_multiply_fusion.1
  5.9 0.1 pad_bitcast_fusion
  6.0 0.7 pad_maximum_fusion.qp_in
  6.8 125.5 %shard_map.136 = bf16[64,2048]{1,0:T(8,128)(2,1)} custom-call(bf16[2,256,128]{2,1,0:T(8,128)(2,1)} %pad_maximum_fusion.1.kvl, bf16[128,128]{1,0:T(8,128)(2,1)} %bitcast.27, bf16[4,256,128]{2,1,0:T(8,128)(2,1)} %pad_maximum_fusion.qp_in, bf16[256,256]{1,0:T(8,128)(2,1)} %rq_in.1, bf16[256,256]{1,0:T(8,128)(2,1)} %fg_in.1, bf16[256,256]{1,0:T(8,128)(2,1)} %rv_in.1, ...), custom_call_target="tpu_custom_call" | custom-call | tf_op jit(solution)/shard_map/pallas_call | solution.py:562
  132.3 1.7 %copy.23 = bf16[64,2048]{1,0:T(8,128)(2,1)} copy(bf16[64,2048]{1,0:T(8,128)(2,1)} %shard_map.136) | data formatting | bytes 524288
  (1 shorter events, 0.0 us)
Async XLA Ops:
  0.0 0.8 copy-start
  0.8 0.8 copy-start.4
  1.5 0.8 copy-start.5
  2.4 0.8 copy-start.3
  3.4 0.7 copy-start.6
  4.1 0.8 copy-start.1
  5.0 0.8 copy-start.2
